TPU v7x, 32 devices: a whole 2x2x4 slice. The times are simulated.
32 devices in a mesh: sp: 16 (over z, y, x), tp: 2 (over core).
Axes of the slice: x: 2, y: 2, z: 4, core: 2. Of those that a mesh axis runs over, the one named last changes fastest.
Arguments:
- residual: bfloat16 [3072, 2048], P(('sp', 'tp')), may hold values from -6 to 6
- queries_narrow: bfloat16 [3072, 512], P('sp', 'tp'), may hold values from -24 to 24
- keys_narrow: bfloat16 [3072, 512], P('sp', 'tp'), may hold values from -24 to 24
- values_narrow: bfloat16 [3072, 512], P('sp', 'tp'), may hold values from -6 to 6
- queries_broad: bfloat16 [3072, 512], P('sp', 'tp'), may hold values from -24 to 24
- keys_broad: bfloat16 [3072, 512], P('sp', 'tp'), may hold values from -24 to 24
- values_broad: bfloat16 [3072, 512], P('sp', 'tp'), may hold values from -6 to 6
- gates_narrow: float32 [3072, 16], P('sp', 'tp'), may hold values from -3072 to 0, as said below
- gates_broad: float32 [3072, 8], P('sp', 'tp'), may hold values from -3072 to 0, as said below
- project_narrow: bfloat16 [512, 2048], P('tp'), may hold values from -0.5 to 0.5
- project_broad: bfloat16 [512, 2048], P('tp'), may hold values from -0.5 to 0.5
- norm_gain: float32 [2048], replicated, may hold values from 0.1 to 1.9
- up_weight: bfloat16 [2048, 8192], P('sp', 'tp'), may hold values from -0.125 to 0.125
- down_weight: bfloat16 [8192, 2048], P('tp', 'sp'), may hold values from -0.0625 to 0.0625
Outputs:
- layer_out: bfloat16 [3072, 2048], P(('sp', 'tp'))
Inputs may be any that keep to these rules, and one draw needn't show every extreme that they name: `gates_narrow`: each head's cumulative log gate never rises from one position to the next. `gates_broad`: each head's cumulative log gate never rises from one position to the next.
All inputs are finite; a program needn't handle non-finite values.
Results may differ from a plain program's by a relative error of at most 0.018.
Values may be sent and summed in bfloat16 or wider, within the bound.
A program may use at most 128 MiB of HBM per device.

v0:
```python
import jax
import jax.numpy as jnp
from jax import lax
from jax.sharding import PartitionSpec as P

A_DIM = 32
B_DIM = 64


def group_update(state, queries, keys, values, query_gates, key_gates, allowed, head_size):
    peak, total, summed = state
    query_count = queries.shape[0]
    key_count = keys.shape[0]
    heads = queries.shape[1] // head_size
    scores = jnp.einsum(
        "qhd,khd->hqk",
        queries.reshape(query_count, heads, head_size),
        keys.reshape(key_count, heads, head_size),
        preferred_element_type=jnp.float32,
    ) * head_size ** (-0.5)
    scores = scores + query_gates.T[:, :, None] - key_gates.T[:, None, :]
    scores = jnp.where(allowed[None], scores, -1e30)
    new_peak = jnp.maximum(peak, jnp.max(scores, axis=-1))
    weights = jnp.exp(scores - new_peak[..., None]) * allowed[None].astype(jnp.float32)
    total = jnp.sum(weights, axis=-1)
    summed = jnp.einsum(
        "hqk,khd->hqd",
        weights.astype(jnp.bfloat16),
        values.reshape(key_count, heads, head_size),
        preferred_element_type=jnp.float32,
    )
    return (new_peak, total, summed)


def empty_state(query_count, heads, head_size):
    return (
        jnp.full((heads, query_count), -1e30, jnp.float32),
        jnp.zeros((heads, query_count), jnp.float32),
        jnp.zeros((heads, query_count, head_size), jnp.float32),
    )


def finish_group(state, head_size):
    peak, total, summed = state
    result = summed / total[..., None]
    return (
        result.transpose(1, 0, 2)
        .reshape(result.shape[1], result.shape[0] * head_size)
        .astype(jnp.bfloat16)
    )


def rms_scaled(mixed, norm_gain):
    mixed_wide = mixed.astype(jnp.float32)
    scale = lax.rsqrt(jnp.mean(mixed_wide * mixed_wide, axis=-1, keepdims=True) + 1e-06)
    return (mixed_wide * scale * norm_gain).astype(jnp.bfloat16)


def local(
    residual,
    queries_narrow,
    keys_narrow,
    values_narrow,
    queries_broad,
    keys_broad,
    values_broad,
    gates_narrow,
    gates_broad,
    project_narrow,
    project_broad,
    norm_gain,
    up_weight,
    down_weight,
):
    local_count = queries_narrow.shape[0]
    table_narrow, table_broad = (
        lax.all_gather(gates_narrow, "sp", axis=0, tiled=True),
        lax.all_gather(gates_broad, "sp", axis=0, tiled=True),
    )
    query_pos = lax.axis_index("sp") * local_count + jnp.arange(local_count, dtype=jnp.int32)
    initial = (
        empty_state(local_count, queries_narrow.shape[1] // A_DIM, A_DIM),
        empty_state(local_count, queries_broad.shape[1] // B_DIM, B_DIM),
    )
    piece_keys_narrow = lax.all_gather(keys_narrow, "sp", axis=0, tiled=True)
    piece_values_narrow = lax.all_gather(values_narrow, "sp", axis=0, tiled=True)
    piece_keys_broad = lax.all_gather(keys_broad, "sp", axis=0, tiled=True)
    piece_values_broad = lax.all_gather(values_broad, "sp", axis=0, tiled=True)
    piece_count = piece_keys_narrow.shape[0]
    key_pos = jnp.arange(piece_count, dtype=jnp.int32)
    allowed = key_pos[None, :] <= query_pos[:, None]
    state_narrow = group_update(
        initial[0],
        queries_narrow,
        piece_keys_narrow,
        piece_values_narrow,
        gates_narrow,
        table_narrow,
        allowed,
        A_DIM,
    )
    state_broad = group_update(
        initial[1],
        queries_broad,
        piece_keys_broad,
        piece_values_broad,
        gates_broad,
        table_broad,
        allowed,
        B_DIM,
    )
    attended_narrow = finish_group(state_narrow, A_DIM)
    attended_broad = finish_group(state_broad, B_DIM)
    projected = lax.psum_scatter(
        (
            jnp.dot(attended_narrow, project_narrow, preferred_element_type=jnp.float32)
            + jnp.dot(attended_broad, project_broad, preferred_element_type=jnp.float32)
        ).astype(jnp.bfloat16),
        "tp",
        scatter_dimension=0,
        tiled=True,
    ).astype(jnp.float32)
    mixed = (residual.astype(jnp.float32) + projected).astype(jnp.bfloat16)
    features = lax.all_gather(rms_scaled(mixed, norm_gain), "tp", axis=0, tiled=True)
    up_total = jnp.dot(
        features,
        lax.all_gather(up_weight, "sp", axis=0, tiled=True),
        preferred_element_type=jnp.float32,
    )
    hidden = jnp.square(jax.nn.relu(up_total)).astype(jnp.bfloat16)
    down_term = jnp.dot(
        hidden,
        lax.all_gather(down_weight, "sp", axis=1, tiled=True),
        preferred_element_type=jnp.float32,
    )
    summed_rows = lax.psum_scatter(
        down_term.astype(jnp.bfloat16), "tp", scatter_dimension=0, tiled=True
    ).astype(jnp.float32)
    return (mixed.astype(jnp.float32) + summed_rows).astype(jnp.bfloat16)


def solution(mesh):
    return jax.shard_map(
        local,
        mesh=mesh,
        in_specs=(
            P(("sp", "tp"), None),
            P("sp", "tp"),
            P("sp", "tp"),
            P("sp", "tp"),
            P("sp", "tp"),
            P("sp", "tp"),
            P("sp", "tp"),
            P("sp", "tp"),
            P("sp", "tp"),
            P("tp", None),
            P("tp", None),
            P(),
            P("sp", "tp"),
            P("tp", "sp"),
        ),
        out_specs=P(("sp", "tp"), None),
        check_vma=False,
    )
```

profile of v0, /device:TPU:0, one launch (start us, length us, event | category | flops | bytes accessed | tf_op | source)
XLA Modules:
  0.0 742.3 jit_solution(3498710460941625432)
XLA Ops:
  6.5 0.7 all-gather.9.cloned.1.call-update
  9.4 1.3 iota_compare_fusion
  10.7 43.5 %all-gather = f32[16,192,8]{1,2,0:T(8,128)S(1)} all-gather(f32[1,192,8]{1,2,0:T(8,128)} %bitcast.59), channel_id=1, replica_groups=mesh['sp'=16,'tp'=2] {'sp'}, dimensions={0}, use_global_device_ids=true | all-gather | bytes 104448 | tf_op jit(solution)/shard_map/all_gather | solution.py:77
  54.3 0.7 reshape.92
  55.0 1.7 copy.29
  56.7 36.3 %all-gather.1 = f32[16,192,4]{1,2,0:T(4,128)S(1)} all-gather(f32[1,192,4]{1,2,0:T(4,128)} %bitcast.65), channel_id=1, replica_groups=mesh['sp'=16,'tp'=2] {'sp'}, dimensions={0}, use_global_device_ids=true | all-gather | bytes 52224 | tf_op jit(solution)/shard_map/all_gather | solution.py:78
  93.1 1.6 copy.33
  94.7 2.6 copy.30
  97.3 7.4 fusion.2
  104.8 6.4 copy-done.4
  111.5 8.6 %fusion = f32[8,192]{1,0:T(8,128)} fusion(f32[8,192,3072]{2,1,0:T(8,128)S(1)} %get-tuple-element.8, f32[192,3072]{1,0:T(8,128)S(1)} %get-tuple-element.6, f32[8,192]{1,0:T(8,128)S(1)} %broadcast_maximum_fusion, f32[8,3072]{1,0:T(8,128)S(1)} %bitcast.53, f32[8,192]{1,0:T(8,128)S(1)} %bitcast.61, pred[192,3072]{1,0:T(8,128)(4,1)S(1)} %copy-done.8), kind=kLoop, calls=%fused_computation.2 | loop fusion | flops 33028608 | bytes 21940224 | tf_op jit(solution)/shard_map/reduce_sum | solution.py:25
  120.2 10.4 %all-gather.13.cloned.1.call-done = bf16[3072,256]{1,0:T(8,128)(2,1)} async-done(((bf16[192,256]{1,0:T(8,128)(2,1)}), bf16[3072,256]{1,0:T(8,128)(2,1)}) %all-gather.13.cloned.1.call-update) | async-done | bytes 1572880 | tf_op jit(solution)/shard_map/all_gather | solution.py:87
  130.6 2.6 copy.34
  133.2 8.0 %fusion.41 = (f32[4,192]{1,0:T(4,128)S(1)}, f32[4,192,3072]{2,1,0:T(8,128)}) fusion(f32[4,3072]{1,0:T(4,128)S(1)} %bitcast.58, f32[4,192]{1,0:T(4,128)} %bitcast.66, bf16[192,4,64]{0,2,1:T(8,128)(2,1)} %bitcast.55, bf16[3072,4,64]{0,2,1:T(8,128)(2,1)} %bitcast.49, pred[192,3072]{1,0:T(8,128)(4,1)} %get-tuple-element.5), kind=kOutput, calls=%fused_computation.43 | convolution fusion | flops 313785600 | bytes 11753472 | tf_op jit(solution)/shard_map/qhd,khd->hqk/dot_general | solution.py:15
  141.1 48.9 %all-gather.11.cloned.1.call-done = bf16[3072,256]{1,0:T(8,128)(2,1)} async-done(((bf16[192,256]{1,0:T(8,128)(2,1)}), bf16[3072,256]{1,0:T(8,128)(2,1)}) %all-gather.11.cloned.1.call-update) | async-done | bytes 1572880 | tf_op jit(solution)/shard_map/all_gather | solution.py:86
  190.1 2.7 copy.32
  192.8 11.0 %fusion.24 = bf16[192,8,32]{0,2,1:T(8,128)(2,1)S(1)} fusion(bf16[3072,8,32]{0,2,1:T(8,128)(2,1)} %bitcast.48, f32[8,192,3072]{2,1,0:T(8,128)} %copy-done.4, f32[192,3072]{1,0:T(8,128)} %copy-done.2, f32[8,192]{1,0:T(8,128)S(1)} %copy-done.15, f32[8,3072]{1,0:T(8,128)S(1)} %bitcast.54, f32[8,192]{1,0:T(8,128)S(1)} %bitcast.62, ...), kind=kOutput, calls=%fused_computation.27 | convolution fusion | flops 335118336 | bytes 23611392 | tf_op jit(solution)/shard_map/hqk,khd->hqd/dot_general | solution.py:26
  203.8 1.6 fusion.42
  205.4 1.8 fusion.6
  207.3 42.1 %all-gather.15.cloned.1.call-done = bf16[3072,256]{1,0:T(8,128)(2,1)} async-done(((bf16[192,256]{1,0:T(8,128)(2,1)}), bf16[3072,256]{1,0:T(8,128)(2,1)}) %all-gather.15.cloned.1.call-update) | async-done | bytes 1572880 | tf_op jit(solution)/shard_map/all_gather | solution.py:88
  249.4 2.6 copy.36
  252.0 6.7 fusion.30
  258.8 1.3 fusion.14
  261.5 5.7 reduce-scatter.3.cloned.1.call-done
  267.1 1.2 fusion.33
  268.4 1.2 fusion.35
  269.6 2.4 all_gather.33
  271.9 190.0 %all-gather.17.cloned.1.call-done = bf16[2048,4096]{1,0:T(8,128)(2,1)} async-done(((bf16[128,4096]{1,0:T(8,128)(2,1)}), bf16[2048,4096]{1,0:T(8,128)(2,1)}) %all-gather.17.cloned.1.call-update) | async-done | bytes 16777232 | tf_op jit(solution)/shard_map/all_gather | solution.py:127
  461.9 250.0 %all-gather.19.cloned.1.call-done = bf16[4096,2048]{1,0:T(8,128)(2,1)} async-done(((bf16[4096,128]{1,0:T(8,128)(2,1)}), bf16[4096,2048]{1,0:T(8,128)(2,1)}) %all-gather.19.cloned.1.call-update) | async-done | bytes 16777232 | tf_op jit(solution)/shard_map/all_gather | solution.py:133
  711.9 15.1 %convolution_convert_fusion = bf16[192,2048]{1,0:T(8,128)(2,1)} fusion(bf16[4096,2048]{1,0:T(8,128)(2,1)} %all-gather.19.cloned.1.call-done, bf16[192,2048]{1,0:T(8,128)(2,1)S(1)} %all_gather.33, bf16[2048,4096]{1,0:T(8,128)(2,1)} %all-gather.17.cloned.1.call-done), kind=kOutput, calls=%fused_computation.18 | convolution fusion | flops 6445203456 | bytes 35127296 | tf_op jit(solution)/shard_map/dot_general | solution.py:131
  727.0 6.5 reduce-scatter.5.cloned.1.call-done
  733.5 1.9 fusion.36
  (65 shorter events, 4.1 us)
Async XLA Ops:
  6.5 197.3 %copy-start = (bf16[256,2048]{1,0:T(8,128)(2,1)S(1)}, bf16[256,2048]{1,0:T(8,128)(2,1)}, u32[]{:S(2)}) copy-start(bf16[256,2048]{1,0:T(8,128)(2,1)} %param.23) | copy-start | bytes 3145732
  6.5 88.2 %all-gather.9.cloned.1.call-start = ((), (), s32[]{:S(2)}) async-start(), calls=%async_computation.2 | async-start | bytes 1671168 | tf_op jit(solution)/shard_map/all_gather | solution.py:85
  7.3 123.3 %all-gather.13.cloned.1.call-start = ((), (), s32[]{:S(2)}) async-start(), calls=%async_computation.4 | async-start | bytes 1671168 | tf_op jit(solution)/shard_map/all_gather | solution.py:87
  8.0 182.0 %all-gather.11.cloned.1.call-start = ((), (), s32[]{:S(2)}) async-start(), calls=%async_computation.3 | async-start | bytes 1671168 | tf_op jit(solution)/shard_map/all_gather | solution.py:86
  8.7 240.7 %all-gather.15.cloned.1.call-start = ((), (), s32[]{:S(2)}) async-start(), calls=%async_computation.5 | async-start | bytes 1671168 | tf_op jit(solution)/shard_map/all_gather | solution.py:88
  9.3 257.8 %reduce-scatter.3.cloned.1.call-start = ((), (), s32[]{:S(2)}) async-start(), calls=%async_computation.6 | async-start | bytes 1179648 | tf_op jit(solution)/shard_map/reduce_scatter | solution.py:114
  10.7 94.0 %copy-start.2 = (f32[192,3072]{1,0:T(8,128)}, f32[192,3072]{1,0:T(8,128)S(1)}, u32[]{:S(2)}) copy-start(f32[192,3072]{1,0:T(8,128)S(1)} %get-tuple-element.6) | copy-start | bytes 7077892
  97.3 14.2 %copy-start.8 = (pred[192,3072]{1,0:T(8,128)(4,1)S(1)}, pred[192,3072]{1,0:T(8,128)(4,1)}, u32[]{:S(2)}) copy-start(pred[192,3072]{1,0:T(8,128)(4,1)} %get-tuple-element.5) | copy-start | bytes 1769476
  97.3 14.2 %copy-start.11 = (f32[3072,8]{0,1:T(8,128)S(1)}, f32[3072,8]{0,1:T(8,128)}, u32[]{:S(2)}) copy-start(f32[3072,8]{0,1:T(8,128)} %reshape.92) | copy-start | bytes 294916
  97.3 14.2 %copy-start.12 = (f32[192,8]{0,1:T(8,128)S(1)}, f32[192,8]{0,1:T(8,128)}, u32[]{:S(2)}) copy-start(f32[192,8]{0,1:T(8,128)} %param.21) | copy-start | bytes 18436
  104.7 6.4 copy-start.4
  104.7 6.8 copy-start.14
  133.2 59.6 %copy-start.9 = (pred[192,3072]{1,0:T(8,128)(4,1)S(1)}, pred[192,3072]{1,0:T(8,128)(4,1)}, u32[]{:S(2)}) copy-start(pred[192,3072]{1,0:T(8,128)(4,1)} %get-tuple-element.5) | copy-start | bytes 1769476
  133.2 59.6 %copy-start.13 = (f32[192,8]{0,1:T(8,128)S(1)}, f32[192,8]{0,1:T(8,128)}, u32[]{:S(2)}) copy-start(f32[192,8]{0,1:T(8,128)} %param.21) | copy-start | bytes 18436
  133.2 59.6 %copy-start.15 = (f32[8,192]{1,0:T(8,128)S(1)}, f32[8,192]{1,0:T(8,128)}, u32[]{:S(2)}) copy-start(f32[8,192]{1,0:T(8,128)} %copy-done.14) | copy-start | bytes 18436
  133.2 59.6 %copy-start.17 = (f32[8,192]{1,0:T(8,128)S(1)}, f32[8,192]{1,0:T(8,128)}, u32[]{:S(2)}) copy-start(f32[8,192]{1,0:T(8,128)} %fusion) | copy-start | bytes 18436
  190.0 15.4 %slice-start = ((s8[9437184]{0:T(1024)(128)(4,1)}), s8[1048576]{0:T(1024)(128)(4,1)S(1)}, s32[]{:S(2)}) async-start(s8[9437184]{0:T(1024)(128)(4,1)} %bitcast.45), calls=%async_computation.10 | async-start | bytes 2097152
  192.8 12.6 %slice-start.1 = ((s8[9437184]{0:T(1024)(128)(4,1)}), s8[4194304]{0:T(1024)(128)(4,1)S(1)}, s32[]{:S(2)}) async-start(s8[9437184]{0:T(1024)(128)(4,1)} %bitcast.45), calls=%async_computation.11 | async-start | bytes 8388608
  192.8 12.6 %slice-start.2 = ((s8[9437184]{0:T(1024)(128)(4,1)}), s8[4194304]{0:T(1024)(128)(4,1)S(1)}, s32[]{:S(2)}) async-start(s8[9437184]{0:T(1024)(128)(4,1)} %bitcast.45), calls=%async_computation.12 | async-start | bytes 8388608
  192.8 12.6 %copy-start.3 = (f32[192,3072]{1,0:T(8,128)S(1)}, f32[192,3072]{1,0:T(8,128)}, u32[]{:S(2)}) copy-start(f32[192,3072]{1,0:T(8,128)} %copy-done.2) | copy-start | bytes 7077892
  207.3 51.5 %copy-start.5 = (f32[192,2048]{1,0:T(8,128)S(1)}, f32[192,2048]{1,0:T(8,128)}, u32[]{:S(2)}) copy-start(f32[192,2048]{1,0:T(8,128)} %fusion.42) | copy-start | bytes 4718596
  207.3 51.5 %copy-start.10 = (bf16[256,2048]{1,0:T(8,128)(2,1)S(1)}, bf16[256,2048]{1,0:T(8,128)(2,1)}, u32[]{:S(2)}) copy-start(bf16[256,2048]{1,0:T(8,128)(2,1)} %param.24) | copy-start | bytes 3145732
  252.0 15.1 %copy-start.6 = (bf16[96,2048]{1,0:T(8,128)(2,1)S(1)}, bf16[96,2048]{1,0:T(8,128)(2,1)}, u32[]{:S(2)}) copy-start(bf16[96,2048]{1,0:T(8,128)(2,1)} %param.14) | copy-start | bytes 1179652
  252.0 16.4 %copy-start.16 = (f32[2048]{0:T(1024)S(1)}, f32[2048]{0:T(1024)}, u32[]{:S(2)}) copy-start(f32[2048]{0:T(1024)} %param.25) | copy-start | bytes 24580
  260.1 201.8 %all-gather.17.cloned.1.call-start = ((), (), s32[]{:S(2)}) async-start(), calls=%async_computation.7 | async-start | bytes 17825792 | tf_op jit(solution)/shard_map/all_gather | solution.py:127
  260.7 451.2 %all-gather.19.cloned.1.call-start = ((), (), s32[]{:S(2)}) async-start(), calls=%async_computation.8 | async-start | bytes 17825792 | tf_op jit(solution)/shard_map/all_gather | solution.py:133
  261.4 472.1 %reduce-scatter.5.cloned.1.call-start = ((), (), s32[]{:S(2)}) async-start(), calls=%async_computation.9 | async-start | bytes 1179648 | tf_op jit(solution)/shard_map/reduce_scatter | solution.py:136
  271.9 461.6 %copy-start.7 = (bf16[96,2048]{1,0:T(8,128)(2,1)S(1)}, bf16[96,2048]{1,0:T(8,128)(2,1)}, u32[]{:S(2)}) copy-start(bf16[96,2048]{1,0:T(8,128)(2,1)} %reduce-scatter.3.cloned.1.call-done) | copy-start | bytes 1179652
  711.9 23.5 %copy-start.1 = (bf16[256,2048]{1,0:T(8,128)(2,1)S(1)}, bf16[256,2048]{1,0:T(8,128)(2,1)}, u32[]{:S(2)}) copy-start(bf16[256,2048]{1,0:T(8,128)(2,1)} %param.23) | copy-start | bytes 3145732
Sparse Core Ops, SparseCore 0:
  10.1 60.9 all-gather.8
  73.8 56.6 all-gather.12
  133.3 56.6 all-gather.10
  192.7 56.7 all-gather.14
  260.2 6.8 reduce-scatter.2
  269.8 192.1 all-gather.16
  464.6 247.2 all-gather.18
  727.2 6.3 reduce-scatter.4
where the time goes:
time: 743 us; the launch traced here: 742 us
  waiting for transfers between devices  557 us (75%)
  blocking collectives  82.2 us (11%)
  matrix products  51.1 us (7%)
  local copies, waits for them, and re-layouts  21.5 us (3%)
  other arithmetic  16.1 us (2%)
  between operations  13.7 us (2%)
    all_gather x1, waiting for transfers between devices, local(): lax.all_gather(down_weight, 'sp', axis=1, tiled=True)  250 us
    all_gather x1, waiting for transfers between devices, local(): lax.all_gather(up_weight, 'sp', axis=0, tiled=True)  190 us
    all_gather x1, waiting for transfers between devices, local(): lax.all_gather(values_narrow, 'sp', axis=0, tiled=True)  48.9 us
    all_gather x1, blocking collectives, local(): lax.all_gather(gates_narrow, 'sp', axis=0, tiled=True)  43.5 us
    all_gather x1, waiting for transfers between devices, local(): piece_values_broad = lax.all_gather(values_broad, 'sp', axis=0, tiled=True)  42.1 us
    all_gather x1, blocking collectives, local(): lax.all_gather(gates_broad, 'sp', axis=0, tiled=True)  36.3 us
    dot_general x2, matrix products, group_update(): jnp.einsum('hqk,khd->hqd', weights.astype(jnp.bfloat16), values.reshape(k...  17.7 us
    dot_general x2, matrix products, group_update(): jnp.einsum('qhd,khd->hqk', queries.reshape(query_count, heads, head_size)...  15.4 us
  transfers between devices with their start and end apart: 8, of which 7 were waited for; matrix products, arithmetic and copies ran while one was open for 7% of the time, Pallas kernels for 0%

commit v1 on v0

--- a/solution.py
+++ b/solution.py
@@ -1,10 +1,21 @@
+import functools
 import jax
 import jax.numpy as jnp
 from jax import lax
 from jax.sharding import PartitionSpec as P
+from jax.lax import all_to_all, axis_size
 
 A_DIM = 32
 B_DIM = 64
+
+
+def refer_masks_up(x_local, axis_key):
+    return jnp.concatenate(
+        all_to_all(jnp.stack([x_local] * axis_size(axis_key), 0), axis_key, 0, 0), 1
+    )
+
+
+derive_values_by_axis = functools.partial(refer_masks_up, axis_key="sp")
 
 
 def group_update(state, queries, keys, values, query_gates, key_gates, allowed, head_size):
@@ -129,9 +140,7 @@
     )
     hidden = jnp.square(jax.nn.relu(up_total)).astype(jnp.bfloat16)
     down_term = jnp.dot(
-        hidden,
-        lax.all_gather(down_weight, "sp", axis=1, tiled=True),
-        preferred_element_type=jnp.float32,
+        hidden, derive_values_by_axis(down_weight), preferred_element_type=jnp.float32
     )
     summed_rows = lax.psum_scatter(
         down_term.astype(jnp.bfloat16), "tp", scatter_dimension=0, tiled=True

time: 743 us -> 840 us (1.13)
  waiting for transfers between devices: 557 us -> 641 us
    all_to_all x0 -> x1, waiting for transfers between devices: none -> 367 us  [refer_masks_up(): all_to_all(jnp.stack([x_local] * axis_size(axis_key), 0), axis_key, 0, 0)]
    all_gather x1 -> x0, waiting for transfers between devices: 250 us -> none  [local(): lax.all_gather(down_weight, 'sp', axis=1, tiled=True)]
    all_gather x1, waiting for transfers between devices: 190 us -> 129 us  [local(): lax.all_gather(up_weight, 'sp', axis=0, tiled=True)]
    reduce_scatter x1, waiting for transfers between devices: 6.5 us -> 40.8 us  [local(): lax.psum_scatter(down_term.astype(jnp.bfloat16), 'tp', scatter_dimension=...]
  transfers between devices with their start and end apart: 8 -> 8, of which waited for: 7 -> 6; matrix products, arithmetic and copies ran while one was open for 7% -> 7% of each run, Pallas kernels for 0% -> 0%
where the time goes in v1:
time: 840 us; the launch traced here: 839 us
  waiting for transfers between devices  641 us (76%)
  blocking collectives  82.1 us (10%)
  matrix products  52.2 us (6%)
  local copies, waits for them, and re-layouts  29 us (3%)
  other arithmetic  16.1 us (2%)
  between operations  13.7 us (2%)
    all_to_all x1, waiting for transfers between devices, refer_masks_up(): all_to_all(jnp.stack([x_local] * axis_size(axis_key), 0), axis_key, 0, 0)  367 us
    all_gather x1, waiting for transfers between devices, local(): lax.all_gather(up_weight, 'sp', axis=0, tiled=True)  129 us
    all_gather x1, waiting for transfers between devices, local(): lax.all_gather(values_narrow, 'sp', axis=0, tiled=True)  48.9 us
    all_gather x1, blocking collectives, local(): lax.all_gather(gates_narrow, 'sp', axis=0, tiled=True)  43.5 us
    all_gather x1, waiting for transfers between devices, local(): piece_values_broad = lax.all_gather(values_broad, 'sp', axis=0, tiled=True)  42.1 us
    reduce_scatter x1, waiting for transfers between devices, local(): lax.psum_scatter(down_term.astype(jnp.bfloat16), 'tp', scatter_dimension=...  40.8 us
    all_gather x1, blocking collectives, local(): lax.all_gather(gates_broad, 'sp', axis=0, tiled=True)  36.2 us
    dot_general x2, matrix products, group_update(): jnp.einsum('hqk,khd->hqd', weights.astype(jnp.bfloat16), values.reshape(k...  17.7 us
  transfers between devices with their start and end apart: 8, of which 6 were waited for; matrix products, arithmetic and copies ran while one was open for 7% of the time, Pallas kernels for 0%

profile of v1, /device:TPU:0, one launch (start us, length us, event | category | flops | bytes accessed | tf_op | source)
XLA Modules:
  0.0 839.4 jit_solution(5525758148933709977)
XLA Ops:
  9.4 1.3 iota_compare_fusion
  10.7 43.5 %all-gather = f32[16,192,8]{1,2,0:T(8,128)S(1)} all-gather(f32[1,192,8]{1,2,0:T(8,128)} %bitcast.62), channel_id=1, replica_groups=mesh['sp'=16,'tp'=2] {'sp'}, dimensions={0}, use_global_device_ids=true | all-gather | bytes 104448 | tf_op jit(solution)/shard_map/all_gather | solution.py:88
  55.0 1.7 copy.30
  56.7 36.2 %all-gather.1 = f32[16,192,4]{1,2,0:T(4,128)S(1)} all-gather(f32[1,192,4]{1,2,0:T(4,128)} %bitcast.68), channel_id=1, replica_groups=mesh['sp'=16,'tp'=2] {'sp'}, dimensions={0}, use_global_device_ids=true | all-gather | bytes 52224 | tf_op jit(solution)/shard_map/all_gather | solution.py:89
  93.0 1.6 copy.34
  94.7 2.6 copy.31
  97.3 7.4 fusion.2
  104.7 6.4 copy-done.4
  111.5 8.6 %fusion = f32[8,192]{1,0:T(8,128)} fusion(f32[8,192,3072]{2,1,0:T(8,128)S(1)} %get-tuple-element.8, f32[192,3072]{1,0:T(8,128)S(1)} %get-tuple-element.6, f32[8,192]{1,0:T(8,128)S(1)} %broadcast_maximum_fusion, f32[8,3072]{1,0:T(8,128)S(1)} %bitcast.56, f32[8,192]{1,0:T(8,128)S(1)} %bitcast.64, pred[192,3072]{1,0:T(8,128)(4,1)S(1)} %copy-done.8), kind=kLoop, calls=%fused_computation.2 | loop fusion | flops 33028608 | bytes 21940224 | tf_op jit(solution)/shard_map/reduce_sum | solution.py:36
  120.1 10.5 %all-gather.12.cloned.1.call-done = bf16[3072,256]{1,0:T(8,128)(2,1)} async-done(((bf16[192,256]{1,0:T(8,128)(2,1)}), bf16[3072,256]{1,0:T(8,128)(2,1)}) %all-gather.12.cloned.1.call-update) | async-done | bytes 1572880 | tf_op jit(solution)/shard_map/all_gather | solution.py:98
  130.6 2.6 copy.35
  133.2 8.0 fusion.41
  141.2 48.9 %all-gather.10.cloned.1.call-done = bf16[3072,256]{1,0:T(8,128)(2,1)} async-done(((bf16[192,256]{1,0:T(8,128)(2,1)}), bf16[3072,256]{1,0:T(8,128)(2,1)}) %all-gather.10.cloned.1.call-update) | async-done | bytes 1572880 | tf_op jit(solution)/shard_map/all_gather | solution.py:97
  190.1 2.7 copy.33
  192.8 11.0 %fusion.24 = bf16[192,8,32]{0,2,1:T(8,128)(2,1)S(1)} fusion(bf16[3072,8,32]{0,2,1:T(8,128)(2,1)} %bitcast.51, f32[8,192,3072]{2,1,0:T(8,128)} %copy-done.4, f32[192,3072]{1,0:T(8,128)} %copy-done.2, f32[8,192]{1,0:T(8,128)S(1)} %copy-done.15, f32[8,3072]{1,0:T(8,128)S(1)} %bitcast.57, f32[8,192]{1,0:T(8,128)S(1)} %bitcast.65, ...), kind=kOutput, calls=%fused_computation.27 | convolution fusion | flops 335118336 | bytes 23611392 | tf_op jit(solution)/shard_map/hqk,khd->hqd/dot_general | solution.py:37
  203.8 1.6 fusion.42
  205.4 1.8 fusion.6
  207.3 42.1 %all-gather.14.cloned.1.call-done = bf16[3072,256]{1,0:T(8,128)(2,1)} async-done(((bf16[192,256]{1,0:T(8,128)(2,1)}), bf16[3072,256]{1,0:T(8,128)(2,1)}) %all-gather.14.cloned.1.call-update) | async-done | bytes 1572880 | tf_op jit(solution)/shard_map/all_gather | solution.py:99
  249.4 2.6 copy.37
  252.0 6.7 fusion.30
  258.7 1.3 fusion.14
  260.1 1.5 copy.38
  261.6 6.0 stack.2
  267.6 5.3 all-to-all-start
  273.6 1.2 fusion.33
  274.8 1.2 fusion.35
  276.0 2.4 all_gather.30
  278.3 366.6 %all-to-all-done = bf16[16,4096,128]{1,2,0:T(8,128)(2,1)} async-done(((bf16[16,4096,128]{1,2,0:T(8,128)(2,1)}), bf16[16,4096,128]{1,2,0:T(8,128)(2,1)}, u32[]{:S(2)}, u32[]{:S(2)}) %all-to-all-start) | async-done | bytes 16777248 | tf_op jit(solution)/shard_map/all_to_all | solution.py:14
  645.0 128.7 %all-gather.16.cloned.1.call-done = bf16[2048,4096]{1,0:T(8,128)(2,1)} async-done(((bf16[128,4096]{1,0:T(8,128)(2,1)}), bf16[2048,4096]{1,0:T(8,128)(2,1)}) %all-gather.16.cloned.1.call-update) | async-done | bytes 16777232 | tf_op jit(solution)/shard_map/all_gather | solution.py:138
  773.7 16.2 %convolution_convert_fusion = bf16[192,2048]{1,0:T(8,128)(2,1)} fusion(bf16[4096,2048]{0,1:T(8,128)(2,1)} %bitcast.19, bf16[192,2048]{1,0:T(8,128)(2,1)S(1)} %all_gather.30, bf16[2048,4096]{1,0:T(8,128)(2,1)} %all-gather.16.cloned.1.call-done), kind=kOutput, calls=%fused_computation.18 | convolution fusion | flops 6445203456 | bytes 35127296 | tf_op jit(solution)/shard_map/dot_general | solution.py:142
  789.9 40.8 %reduce-scatter.5.cloned.1.call-done = bf16[96,2048]{1,0:T(8,128)(2,1)} async-done(((bf16[192,2048]{1,0:T(8,128)(2,1)}), bf16[96,2048]{1,0:T(8,128)(2,1)}) %reduce-scatter.5.cloned.1.call-update) | async-done | bytes 393232 | tf_op jit(solution)/shard_map/reduce_scatter | solution.py:145
  830.7 1.9 fusion.36
  (66 shorter events, 4.8 us)
Async XLA Ops:
  6.5 197.3 %copy-start = (bf16[256,2048]{1,0:T(8,128)(2,1)S(1)}, bf16[256,2048]{1,0:T(8,128)(2,1)}, u32[]{:S(2)}) copy-start(bf16[256,2048]{1,0:T(8,128)(2,1)} %param.23) | copy-start | bytes 3145732
  6.5 88.1 %all-gather.8.cloned.1.call-start = ((), (), s32[]{:S(2)}) async-start(), calls=%async_computation.3 | async-start | bytes 1671168 | tf_op jit(solution)/shard_map/all_gather | solution.py:96
  7.3 123.3 %all-gather.12.cloned.1.call-start = ((), (), s32[]{:S(2)}) async-start(), calls=%async_computation.5 | async-start | bytes 1671168 | tf_op jit(solution)/shard_map/all_gather | solution.py:98
  8.0 182.0 %all-gather.10.cloned.1.call-start = ((), (), s32[]{:S(2)}) async-start(), calls=%async_computation.4 | async-start | bytes 1671168 | tf_op jit(solution)/shard_map/all_gather | solution.py:97
  8.7 240.7 %all-gather.14.cloned.1.call-start = ((), (), s32[]{:S(2)}) async-start(), calls=%async_computation.6 | async-start | bytes 1671168 | tf_op jit(solution)/shard_map/all_gather | solution.py:99
  9.3 264.2 %reduce-scatter.3.cloned.1.call-start = ((), (), s32[]{:S(2)}) async-start(), calls=%async_computation.7 | async-start | bytes 1179648 | tf_op jit(solution)/shard_map/reduce_scatter | solution.py:125
  10.7 94.0 %copy-start.2 = (f32[192,3072]{1,0:T(8,128)}, f32[192,3072]{1,0:T(8,128)S(1)}, u32[]{:S(2)}) copy-start(f32[192,3072]{1,0:T(8,128)S(1)} %get-tuple-element.6) | copy-start | bytes 7077892
  97.3 14.2 %copy-start.8 = (pred[192,3072]{1,0:T(8,128)(4,1)S(1)}, pred[192,3072]{1,0:T(8,128)(4,1)}, u32[]{:S(2)}) copy-start(pred[192,3072]{1,0:T(8,128)(4,1)} %get-tuple-element.5) | copy-start | bytes 1769476
  97.3 14.2 %copy-start.11 = (f32[3072,8]{0,1:T(8,128)S(1)}, f32[3072,8]{0,1:T(8,128)}, u32[]{:S(2)}) copy-start(f32[3072,8]{0,1:T(8,128)} %reshape.102) | copy-start | bytes 294916
  97.3 14.2 %copy-start.12 = (f32[192,8]{0,1:T(8,128)S(1)}, f32[192,8]{0,1:T(8,128)}, u32[]{:S(2)}) copy-start(f32[192,8]{0,1:T(8,128)} %param.21) | copy-start | bytes 18436
  104.7 6.4 copy-start.4
  104.7 6.8 copy-start.14
  133.2 59.6 %copy-start.9 = (pred[192,3072]{1,0:T(8,128)(4,1)S(1)}, pred[192,3072]{1,0:T(8,128)(4,1)}, u32[]{:S(2)}) copy-start(pred[192,3072]{1,0:T(8,128)(4,1)} %get-tuple-element.5) | copy-start | bytes 1769476
  133.2 59.6 %copy-start.13 = (f32[192,8]{0,1:T(8,128)S(1)}, f32[192,8]{0,1:T(8,128)}, u32[]{:S(2)}) copy-start(f32[192,8]{0,1:T(8,128)} %param.21) | copy-start | bytes 18436
  133.2 59.6 %copy-start.15 = (f32[8,192]{1,0:T(8,128)S(1)}, f32[8,192]{1,0:T(8,128)}, u32[]{:S(2)}) copy-start(f32[8,192]{1,0:T(8,128)} %copy-done.14) | copy-start | bytes 18436
  133.2 59.6 %copy-start.17 = (f32[8,192]{1,0:T(8,128)S(1)}, f32[8,192]{1,0:T(8,128)}, u32[]{:S(2)}) copy-start(f32[8,192]{1,0:T(8,128)} %fusion) | copy-start | bytes 18436
  190.1 15.4 %slice-start = ((s8[9437184]{0:T(1024)(128)(4,1)}), s8[1048576]{0:T(1024)(128)(4,1)S(1)}, s32[]{:S(2)}) async-start(s8[9437184]{0:T(1024)(128)(4,1)} %bitcast.48), calls=%async_computation.10 | async-start | bytes 2097152
  192.8 12.6 %slice-start.1 = ((s8[9437184]{0:T(1024)(128)(4,1)}), s8[4194304]{0:T(1024)(128)(4,1)S(1)}, s32[]{:S(2)}) async-start(s8[9437184]{0:T(1024)(128)(4,1)} %bitcast.48), calls=%async_computation.11 | async-start | bytes 8388608
  192.8 12.6 %slice-start.2 = ((s8[9437184]{0:T(1024)(128)(4,1)}), s8[4194304]{0:T(1024)(128)(4,1)S(1)}, s32[]{:S(2)}) async-start(s8[9437184]{0:T(1024)(128)(4,1)} %bitcast.48), calls=%async_computation.12 | async-start | bytes 8388608
  192.8 12.6 %copy-start.3 = (f32[192,3072]{1,0:T(8,128)S(1)}, f32[192,3072]{1,0:T(8,128)}, u32[]{:S(2)}) copy-start(f32[192,3072]{1,0:T(8,128)} %copy-done.2) | copy-start | bytes 7077892
  207.3 51.4 %copy-start.5 = (f32[192,2048]{1,0:T(8,128)S(1)}, f32[192,2048]{1,0:T(8,128)}, u32[]{:S(2)}) copy-start(f32[192,2048]{1,0:T(8,128)} %fusion.42) | copy-start | bytes 4718596
  207.3 51.4 %copy-start.10 = (bf16[256,2048]{1,0:T(8,128)(2,1)S(1)}, bf16[256,2048]{1,0:T(8,128)(2,1)}, u32[]{:S(2)}) copy-start(bf16[256,2048]{1,0:T(8,128)(2,1)} %param.24) | copy-start | bytes 3145732
  267.6 6.0 copy-start.6
  267.6 7.2 copy-start.16
  267.6 377.4 %all-to-all-start = ((bf16[16,4096,128]{1,2,0:T(8,128)(2,1)}), bf16[16,4096,128]{1,2,0:T(8,128)(2,1)}, u32[]{:S(2)}, u32[]{:S(2)}) async-start(bf16[16,4096,128]{1,2,0:T(8,128)(2,1)} %stack.2), calls=%async_computation.1 | async-start | bytes 33554432 | tf_op jit(solution)/shard_map/all_to_all | solution.py:14
  272.9 500.8 %all-gather.16.cloned.1.call-start = ((), (), s32[]{:S(2)}) async-start(), calls=%async_computation.8 | async-start | bytes 17825792 | tf_op jit(solution)/shard_map/all_gather | solution.py:138
  273.5 557.2 %reduce-scatter.5.cloned.1.call-start = ((), (), s32[]{:S(2)}) async-start(), calls=%async_computation.9 | async-start | bytes 1179648 | tf_op jit(solution)/shard_map/reduce_scatter | solution.py:145
  773.7 57.0 %copy-start.7 = (bf16[96,2048]{1,0:T(8,128)(2,1)S(1)}, bf16[96,2048]{1,0:T(8,128)(2,1)}, u32[]{:S(2)}) copy-start(bf16[96,2048]{1,0:T(8,128)(2,1)} %reduce-scatter.3.cloned.1.call-done) | copy-start | bytes 1179652
  773.7 58.9 %copy-start.1 = (bf16[256,2048]{1,0:T(8,128)(2,1)S(1)}, bf16[256,2048]{1,0:T(8,128)(2,1)}, u32[]{:S(2)}) copy-start(bf16[256,2048]{1,0:T(8,128)(2,1)} %param.23) | copy-start | bytes 3145732
Sparse Core Ops, SparseCore 0:
  10.1 60.9 all-gather.7
  73.8 56.6 all-gather.11
  133.3 56.6 all-gather.9
  192.7 56.7 all-gather.13
  260.2 6.8 reduce-scatter.2
  276.2 497.4 all-gather.15
  790.0 40.5 reduce-scatter.4
